TPU v7x, 32 devices: a whole 2x2x4 slice. The times are simulated.
32 devices in a mesh: pp: 4 (over z), fs: 4 (over y, x), tp: 2 (over core).
Axes of the slice: x: 2, y: 2, z: 4, core: 2. Of those that a mesh axis runs over, the one named last changes fastest.
Arguments:
- tokens: bfloat16 [4, 512, 1024], P('pp', 'fs', 'tp'), parts along dimension 1, may hold values from -640 to 640
- query_matrix: bfloat16 [4, 1024, 1024], P('pp', None, 'tp'), may hold values from -0.1875 to 0.1875
- key_matrix: bfloat16 [4, 1024, 1024], P('pp', None, 'tp'), may hold values from -0.1875 to 0.1875
- value_matrix: bfloat16 [4, 1024, 1024], P('pp', None, 'tp'), may hold values from -0.1875 to 0.1875
- output_gate_weight: bfloat16 [4, 1024, 1024], P('pp', None, 'tp'), may hold values from -0.1875 to 0.1875
- strength_weight: bfloat16 [4, 1024, 8], P('pp', None, 'tp'), may hold values from -0.1875 to 0.1875
- decay_input_weight: bfloat16 [4, 1024, 8], P('pp', None, 'tp'), may hold values from -0.1875 to 0.1875
- decay_scale_table: float32 [4, 8], P('pp', 'tp'), may hold values from 0.00078125 to 0.234375
- log_spike_decay: float32 [4, 128, 8], P('pp', None, 'tp'), may hold values from -2.1 to 0
- head_norm_gain: float32 [4, 1024], P('pp', 'tp'), may hold values from 0.1 to 1.9
- closing_norm_gain: float32 [1024], P('tp'), may hold values from 0.1 to 1.9
Outputs:
- normalized: bfloat16 [4, 512, 1024], P('pp', 'fs', 'tp'), parts along dimension 1
There are 4 independent parts, one for each index of `fs`. A program takes and returns all parts, laid end to end along the dimension named above; an argument that names none is the same for every part. Nothing has to cross between parts.
All inputs are finite; a program needn't handle non-finite values.
Results may differ from a plain program's by a relative error of at most 0.012.
Values may be sent and summed in bfloat16 or wider, within the bound.
A program may use at most 64 MiB of HBM per device.

v0:
```python
import functools
import jax
import jax.numpy as jnp
from jax import lax
from jax.experimental import pallas as pl
from jax.experimental.pallas import tpu as pltpu
from jax.sharding import PartitionSpec as P

epsilon = 1e-06
F32 = jnp.float32
BF16 = jnp.bfloat16
MESH = pl.DeviceIdType.MESH
NT = (((1,), (1,)), ((), ()))


def silu(a):
    return a * (0.5 + 0.5 * jnp.tanh(0.5 * a))


def dot(a, b):
    return jnp.dot(a.astype(BF16), b.astype(BF16), preferred_element_type=F32)


def stack_kernel(
    stages,
    group,
    size,
    tokens,
    query_hbm,
    key_hbm,
    value_hbm,
    gate_hbm,
    strength_hbm,
    decay_in_hbm,
    decay_speed_hbm,
    spike_hbm,
    gain_hbm,
    closing_hbm,
    out,
    strength,
    decay_in,
    decay_speed,
    spike,
    gain,
    closing_gain,
    weights,
    acc,
    squares_own,
    beta_own,
    decay_own,
    decay_wide,
    speed_wide,
    spike_wide,
    xin,
    xout,
    yin,
    past_key,
    past_value,
    past_fade,
    part_mine,
    part_other,
    w_sem,
    small_sem,
    token_sem,
    go_sem,
    in_sem,
    entry_sem,
    fwd_send,
    fwd_recv,
    out_send,
    y_recv,
    part_send,
    part_recv,
):
    stage = lax.axis_index("pp")
    core = lax.axis_index("tp")
    last = stages - 1
    length, half = tokens.shape
    heads = xout.shape[1]
    width = half // heads
    model_width = group * half
    others = range(1, group)
    spans = [slice(start, start + size) for start in range(0, length, size)]

    def peer(d):
        return lax.rem(core + d, group)

    barrier = pltpu.get_barrier_semaphore()
    for d in range(1, stages):
        pl.semaphore_signal(
            barrier, inc=1, device_id={"pp": lax.rem(stage + d, stages)}, device_id_type=MESH
        )
    for d in others:
        pl.semaphore_signal(barrier, inc=1, device_id={"tp": peer(d)}, device_id_type=MESH)

    def token_copy(h, target):
        return pltpu.make_async_copy(
            tokens.at[:, h * width : (h + 1) * width], target, token_sem.at[h]
        )

    @pl.when(stage == 0)
    def _():
        for h in range(heads):
            token_copy(h, xin.at[0, core * heads + h]).start()

    @pl.when(stage > 0)
    def _():
        for h in range(heads):
            token_copy(h, xout.at[stages, h]).start()

    small_loads = [
        pltpu.make_async_copy(a, b, small_sem.at[i])
        for i, (a, b) in enumerate(
            (
                (strength_hbm, strength),
                (decay_in_hbm, decay_in),
                (decay_speed_hbm, decay_speed),
                (spike_hbm, spike),
                (gain_hbm, gain),
                (closing_hbm, closing_gain),
            )
        )
    ]
    for load in small_loads:
        load.start()
    loads = [
        pltpu.make_async_copy(ref, weights.at[i], w_sem.at[i])
        for i, ref in enumerate((key_hbm, query_hbm, value_hbm, gate_hbm))
    ]
    for load in loads:
        load.start()

    pl.semaphore_wait(barrier, stages + group - 2)

    def entry_copy(h, span):
        return pltpu.make_async_remote_copy(
            src_ref=xout.at[stages, h, span],
            dst_ref=xin.at[stage, core * heads + h, span],
            send_sem=entry_sem.at[span.start // size, h],
            recv_sem=in_sem.at[stage, span.start // size, h],
            device_id={"pp": 0},
            device_id_type=MESH,
        )

    def next_copy(m, h, span):
        return pltpu.make_async_remote_copy(
            src_ref=xout.at[m, h, span],
            dst_ref=xin.at[m, core * heads + h, span],
            send_sem=out_send.at[m, span.start // size, h],
            recv_sem=in_sem.at[m, span.start // size, h],
            device_id={"pp": lax.rem(stage + 1, stages)},
            device_id_type=MESH,
        )

    def exit_copy(m, h, span):
        return pltpu.make_async_remote_copy(
            src_ref=xout.at[m, h, span],
            dst_ref=yin.at[h, span],
            send_sem=out_send.at[m, span.start // size, h],
            recv_sem=y_recv.at[span.start // size, h],
            device_id={"pp": m},
            device_id_type=MESH,
        )

    def forward_copy(m, d, h, span):
        return pltpu.make_async_remote_copy(
            src_ref=xin.at[m, core * heads + h, span],
            dst_ref=xin.at[m, core * heads + h, span],
            send_sem=fwd_send.at[m, d - 1, span.start // size, h],
            recv_sem=fwd_recv.at[m, d - 1, span.start // size, h],
            device_id={"tp": peer(d)},
            device_id_type=MESH,
        )

    @pl.when(stage == 0)
    def _():
        for h in range(heads):
            token_copy(h, xin.at[0, core * heads + h]).wait()

    early = max(heads - 2, 0)

    @pl.when(stage > 0)
    def _():
        for h in range(heads):
            token_copy(h, xout.at[stages, h]).wait()

        @pl.when(stage > 1)
        def _():
            pl.semaphore_wait(go_sem, 1)

        for span in spans:
            for h in range(heads):
                entry_copy(h, span).start()
        entry_copy(early, spans[-1]).wait_send()

        @pl.when(stage < last)
        def _():
            pl.semaphore_signal(
                go_sem, inc=1, device_id={"pp": lax.rem(stage + 1, stages)}, device_id_type=MESH
            )

    for load in small_loads:
        load.wait()
    side = min(length // size, heads)
    groups = heads // side
    lanes = side * size
    block = min(16, size)
    pieces = size // block
    every = range(groups)
    spike_columns = jnp.concatenate(
        [spike[...], jnp.zeros((length - heads, length), F32)], axis=0
    ).T
    for g in every:
        for p in range(side):
            h = g + p * groups
            at = slice(g * lanes + p * size, g * lanes + (p + 1) * size)
            speed_wide[:, at] = jnp.broadcast_to(decay_speed[:, h : h + 1], (1, size))
        spread = jnp.broadcast_to(spike_columns[:, g : g + 1], (length, lanes))
        for p in range(1, side):
            h = g + p * groups
            lane = lax.broadcasted_iota(jnp.int32, (length, lanes), 1)
            other = jnp.broadcast_to(spike_columns[:, h : h + 1], (length, lanes))
            spread = jnp.where(lane >= p * size, other, spread)
        spike_wide[:, g * lanes : (g + 1) * lanes] = spread
    tile = min(256, model_width)
    same = lax.broadcasted_iota(jnp.int32, (tile, tile), 0) == lax.broadcasted_iota(
        jnp.int32, (tile, tile), 1
    )
    identity = jnp.where(same, 1.0, 0.0).astype(BF16)
    for start in range(0, model_width, tile):
        part = decay_in[:heads, start : start + tile].astype(F32)
        wide = jnp.concatenate(
            [
                jnp.broadcast_to(part[g + p * groups : g + p * groups + 1], (size, tile))
                for g in every
                for p in range(side)
            ],
            axis=0,
        ).astype(BF16)
        decay_wide[start : start + tile, :] = lax.dot_general(
            identity, wide, NT, preferred_element_type=F32
        ).astype(BF16)

    def gather(m, which, span):
        return jnp.concatenate([xin[m, which * heads + h, span] for h in range(heads)], axis=1)

    def glance(x, which):
        own = pl.ds(pl.multiple_of(which * half, half), half)
        wide = x.astype(F32)
        squares = jnp.sum(wide * wide, axis=1, keepdims=True)
        decay = dot(x, decay_wide[own, :])
        beta = lax.dot_general(x, strength[:, own], NT, preferred_element_type=F32)
        return squares, decay, beta[:, :heads]

    def project(x, which):
        own = pl.ds(pl.multiple_of(which * half, half), half)
        return [dot(x, weights[i, own, :]) for i in range(4)]

    def begin(m, span):
        x = gather(m, core, span)
        squares, decay, beta = glance(x, core)
        squares_own[span] = jnp.broadcast_to(squares, (size, width))
        decay_own[span] = decay
        beta_own[span] = beta
        for i, a in enumerate(project(x, core)):
            acc[i, span] = a

    def chunk(m, span, keep, use, between):
        squares = squares_own[span, :1]
        decay = decay_own[span]
        beta = beta_own[span]
        for d in others:
            for h in range(heads):
                forward_copy(m, d, h, span).wait_recv()
            source = peer(group - d)
            x = gather(m, source, span)
            squares_other, decay_other, beta_other = glance(x, source)
            squares = squares + squares_other
            decay = decay + decay_other
            beta = beta + beta_other
            for h in range(heads):
                forward_copy(m, d, h, span).wait_send()
            mats = project(x, source)
            if d < group - 1:
                for i in range(4):
                    acc[i, span] += mats[i]
        inv_rms = lax.rsqrt(squares / model_width + epsilon)

        row = lax.broadcasted_iota(jnp.int32, (size, lanes), 0)
        lane = lax.broadcasted_iota(jnp.int32, (size, lanes), 1)
        column = lane % size
        band = (lax.broadcasted_iota(jnp.int32, (8, lanes), 1) % size) // block

        beta = 1.0 / (1.0 + jnp.exp(-beta * inv_rms))
        pre = decay * inv_rms
        softplus = jnp.maximum(pre, 0.0) + jnp.log(1.0 + jnp.exp(-jnp.abs(pre)))
        log_decay = spike_wide[span, :] - speed_wide[...] * softplus
        lower = jnp.where(
            lax.broadcasted_iota(jnp.int32, (size, size), 0)
            >= lax.broadcasted_iota(jnp.int32, (size, size), 1),
            1.0,
            0.0,
        ).astype(BF16)
        high = log_decay.astype(BF16)
        rest = log_decay - high.astype(F32)
        after = jnp.concatenate([row > column] * groups, axis=1)

        def total(mask):
            picked = (jnp.where(after, a.astype(F32), 0.0) if mask else a for a in (high, rest))
            return sum(dot(lower, a) for a in picked)

        since = total(True)
        if use:
            whole = total(False)

        def packed(which, g):
            return jnp.concatenate([which[g + p * groups] for p in range(side)], axis=1)

        def apart(which, g):
            empty = jnp.zeros_like(which[0])
            return jnp.concatenate(
                [
                    jnp.concatenate(
                        [which[g + p * groups] if s == p else empty for s in range(side)], axis=1
                    )
                    for p in range(side)
                ],
                axis=0,
            )

        def stacked(square):
            if side == 1:
                return square
            return jnp.concatenate(
                [jnp.where(lane // size == p, square, jnp.zeros_like(square)) for p in range(side)],
                axis=0,
            )

        def columns(i, h):
            part = slice(h * width, (h + 1) * width)
            return (acc[i, span, part] + mats[i][:, part]) * inv_rms

        def norm(a):
            return lax.rsqrt(jnp.sum(a * a, axis=1, keepdims=True) + epsilon)

        keys = [silu(columns(0, h)) for h in range(heads)]
        rounded_keys = [a.astype(BF16) for a in keys]
        queries = [silu(columns(1, h)) for h in range(heads)]
        rounded_queries = [a.astype(BF16) for a in queries]
        gram = []
        for g in every:
            left = jnp.concatenate([packed(rounded_keys, g), packed(rounded_queries, g)], axis=0)
            gram.append(
                lax.dot_general(left, apart(rounded_keys, g), NT, preferred_element_type=F32)
            )
        key_scale = [norm(a) for a in keys]
        query_scale = [norm(a) * width ** (-0.5) for a in queries]
        force = [beta[:, h : h + 1] * key_scale[h] for h in range(heads)]
        weight = [force[h] * key_scale[h] for h in range(heads)]
        values = [silu(columns(2, h)) * force[h] for h in range(heads)]

        def stretch(parts, g):
            out = jnp.broadcast_to(parts[g], (size, lanes))
            for p in range(1, side):
                out = jnp.where(
                    lane >= p * size, jnp.broadcast_to(parts[g + p * groups], (size, lanes)), out
                )
            return out

        def section(wide, g):
            return wide[:, g * lanes : (g + 1) * lanes]

        decayed = [jnp.where(row >= column, jnp.exp(section(since, g)), 0.0) for g in every]
        scale = [stretch(weight, g) for g in every]
        system = [
            jnp.where(row > column, gram[g][:size] * decayed[g], 0.0) * scale[g] for g in every
        ]
        scores = [(gram[g][size:] * decayed[g]).astype(BF16) for g in every]

        before = None
        if use:
            past_keys = [past_key[h] for h in range(heads)]
            past_values = [past_value[h] for h in range(heads)]
            before = []
            for g in every:
                left = jnp.concatenate(
                    [packed(rounded_keys, g), packed(rounded_queries, g)], axis=0
                )
                cross = lax.dot_general(left, apart(past_keys, g), NT, preferred_element_type=F32)
                fade = jnp.exp(section(whole, g) + past_fade[g : g + 1, :])
                cross = (cross * jnp.concatenate([fade, fade], axis=0)).astype(BF16)
                before.append(
                    jnp.dot(cross, apart(past_values, g), preferred_element_type=F32)
                )
            for g in every:
                for p in range(side):
                    h = g + p * groups
                    part = slice(p * width, (p + 1) * width)
                    values[h] = values[h] - weight[h] * before[g][:size, part]

        tiles = block // 8
        inverse = []
        for g in every:
            compact = []
            for t in range(tiles):
                tile = system[g][t * 8 : t * 8 + 8]
                for r in range(1, pieces):
                    at = r * block + t * 8
                    tile = jnp.where(band == r, system[g][at : at + 8], tile)
                compact.append(tile)
            inner = lax.broadcasted_iota(jnp.int32, (8, lanes), 1) % block
            down_rows = lax.broadcasted_iota(jnp.int32, (8, lanes), 0)
            solved = [
                jnp.where(down_rows + t * 8 == inner, 1.0, 0.0).astype(F32) for t in range(tiles)
            ]
            start_of = lax.broadcasted_iota(jnp.int32, (8, lanes), 1) - inner
            for j in range(block - 1):
                source = jnp.broadcast_to(
                    solved[j // 8][j % 8 : j % 8 + 1, :], (8, lanes)
                )
                for t in range((j + 1) // 8, tiles):
                    factor = jnp.take_along_axis(
                        compact[t], start_of + j, axis=1, mode="promise_in_bounds"
                    )
                    solved[t] = solved[t] - factor * source
            inverse.append(
                jnp.concatenate(
                    [
                        jnp.where(band == r, solved[t], 0.0).astype(F32)
                        for r in range(pieces)
                        for t in range(tiles)
                    ],
                    axis=0,
                ).astype(BF16)
            )
        between()
        update = [dot(inverse[g], apart([a.astype(BF16) for a in values], g)) for g in every]

        def split(wide):
            return [
                wide[h % groups][:, (h // groups) * width : (h // groups + 1) * width].astype(BF16)
                for h in range(heads)
            ]

        if pieces > 1:
            outside = row // block != column // block
            chain = [
                dot(inverse[g], stacked(jnp.where(outside, system[g], 0.0).astype(BF16)))
                for g in every
            ]
            sign = -1.0
            done = 1
            while done < pieces:
                rounded = [chain[g].astype(BF16) for g in every]
                current = split(update)
                update = [
                    update[g] + sign * dot(rounded[g], apart(current, g)) for g in every
                ]
                done *= 2
                sign = 1.0
                if done < pieces:
                    chain = [dot(rounded[g], stacked(rounded[g])) for g in every]
        final = split(update)
        mixed = [dot(scores[g], apart(final, g)) for g in every]
        if use:
            mixed = [mixed[g] + before[g][size:] for g in every]
        for h in range(heads):
            part = slice((h // groups) * width, (h // groups + 1) * width)
            raw = mixed[h % groups][:, part]
            gate = silu(columns(3, h)) * gain[:, h * width : (h + 1) * width]
            mean = jnp.mean(raw * raw, axis=1, keepdims=True)
            unit = query_scale[h]
            head_out = raw * (unit * lax.rsqrt(unit * unit * mean + epsilon)) * gate
            x = xin[m, core * heads + h, span].astype(F32)
            xout[m, h, span] = (x + head_out.astype(BF16).astype(F32)).astype(BF16)
        if keep:
            for h in range(heads):
                past_key[h] = rounded_keys[h]
                past_value[h] = final[h]
            for g in every:
                past_fade[g : g + 1, :] = section(since, g)[size - 1 : size, :]

    def arrive(m, span):
        for h in range(heads):
            next_copy(m, h, span).wait_recv()
            for d in others:
                forward_copy(m, d, h, span).start()

    def enter(span):
        @pl.when(stage > 0)
        def _():
            arrive(0, span)

        @pl.when(stage == 0)
        def _():
            for h in range(heads):
                for d in others:
                    forward_copy(0, d, h, span).start()

    def leave(m, span):
        @pl.when(stage < last)
        def _():
            for h in range(heads):
                next_copy(m, h, span).start()

        @pl.when((stage == last) & (m < last))
        def _():
            for h in range(heads):
                exit_copy(m, h, span).start()

    def step(m, _):
        for i, span in enumerate(spans):

            def between(i=i):
                if i + 1 < len(spans):
                    following, ahead = m, spans[i + 1]

                    @pl.when((stage > 0) | (m > 0))
                    def _():
                        arrive(following, ahead)

                else:
                    following, ahead = lax.rem(m + 1, stages), spans[0]

                    @pl.when(m < last)
                    def _():
                        arrive(following, ahead)

                begin(following, ahead)

            chunk(m, span, keep=i + 1 < len(spans), use=i > 0, between=between)
            leave(m, span)
        return 0

    enter(spans[0])
    for load in loads:
        load.wait()
    begin(0, spans[0])

    @pl.when(stage == 0)
    def _():
        for span in spans[1:]:
            for h in range(heads):
                for d in others:
                    forward_copy(0, d, h, span).start()

    lax.fori_loop(0, stages, step, 0)

    @pl.when(stage == last)
    def _():
        for h in range(heads):
            yin[h] = xout[last, h]

    @pl.when(stage < last)
    def _():
        for span in spans:
            for h in range(heads):
                exit_copy(0, h, span).wait_recv()

    final = [yin[h].astype(F32) for h in range(heads)]
    total = sum(jnp.sum(a * a, axis=1, keepdims=True) for a in final)
    part_mine[...] = jnp.broadcast_to(total, part_mine.shape)
    part_copies = [
        pltpu.make_async_remote_copy(
            src_ref=part_mine,
            dst_ref=part_other.at[d - 1],
            send_sem=part_send.at[d - 1],
            recv_sem=part_recv.at[d - 1],
            device_id={"tp": peer(d)},
            device_id_type=MESH,
        )
        for d in others
    ]
    for copy in part_copies:
        copy.start()

    @pl.when(stage > 0)
    def _():
        for span in spans:
            for h in range(heads):
                if h != early or span is not spans[-1]:
                    entry_copy(h, span).wait_send()

    def drain(m, _):
        @pl.when((stage < last) | (m < last))
        def _():
            for span in spans:
                for h in range(heads):
                    next_copy(m, h, span).wait_send()

        return 0

    lax.fori_loop(0, stages, drain, 0)
    total = part_mine[...]
    for copy in part_copies:
        copy.wait()
    for d in others:
        total = total + part_other[d - 1]
    inv_rms = lax.rsqrt(total / model_width + epsilon)
    for h in range(heads):
        part = slice(h * width, (h + 1) * width)
        out[:, part] = (final[h] * inv_rms * closing_gain[:, part]).astype(BF16)


def on_device(
    stages,
    group,
    tokens,
    query_matrix,
    key_matrix,
    value_matrix,
    output_gate_weight,
    strength_weight,
    decay_input_weight,
    decay_scale_table,
    log_spike_decay,
    head_norm_gain,
    closing_norm_gain,
):
    _, length, half = tokens.shape
    heads = strength_weight.shape[-1]
    width = half // heads
    parts = 2 if heads % 2 == 0 else 1
    size = length // parts

    def rows_of(weight):
        return jnp.pad(weight[0].T, ((0, 1), (0, 0))) if heads == 1 else weight[0].T

    vmem = pl.BlockSpec(memory_space=pltpu.VMEM)
    anywhere = pl.BlockSpec(memory_space=pltpu.HBM)
    dma = pltpu.SemaphoreType.DMA
    result = pl.pallas_call(
        functools.partial(stack_kernel, stages, group, size),
        out_shape=pltpu.VMEM((length, half), BF16),
        in_specs=[anywhere] * 11,
        out_specs=vmem,
        scratch_shapes=[
            pltpu.VMEM((max(heads, 2), group * half), BF16),
            pltpu.VMEM((max(heads, 2), group * half), BF16),
            pltpu.VMEM((1, heads), F32),
            pltpu.VMEM((heads, length), F32),
            pltpu.VMEM((1, half), F32),
            pltpu.VMEM((1, half), F32),
            pltpu.VMEM((4, group * half, half), BF16),
            pltpu.VMEM((4, length, half), F32),
            pltpu.VMEM((length, width), F32),
            pltpu.VMEM((length, heads), F32),
            pltpu.VMEM((length, heads * size), F32),
            pltpu.VMEM((group * half, heads * size), BF16),
            pltpu.VMEM((1, heads * size), F32),
            pltpu.VMEM((length, heads * size), F32),
            pltpu.VMEM((stages, group * heads, length, width), BF16),
            pltpu.VMEM((stages + 1, heads, length, width), BF16),
            pltpu.VMEM((heads, length, width), BF16),
            pltpu.VMEM((heads, size, width), BF16),
            pltpu.VMEM((heads, size, width), BF16),
            pltpu.VMEM((8, length), F32),
            pltpu.VMEM((length, width), F32),
            pltpu.VMEM((group - 1, length, width), F32),
            dma((4,)),
            dma((6,)),
            dma((heads,)),
            pltpu.SemaphoreType.REGULAR,
            dma((stages, parts, heads)),
            dma((parts, heads)),
            dma((stages, group - 1, parts, heads)),
            dma((stages, group - 1, parts, heads)),
            dma((stages, parts, heads)),
            dma((parts, heads)),
            dma((group - 1,)),
            dma((group - 1,)),
        ],
        compiler_params=pltpu.CompilerParams(
            collective_id=0, has_side_effects=True, vmem_limit_bytes=60 * 1024 * 1024
        ),
    )(
        tokens[0],
        query_matrix[0],
        key_matrix[0],
        value_matrix[0],
        output_gate_weight[0],
        rows_of(strength_weight),
        rows_of(decay_input_weight),
        decay_scale_table,
        log_spike_decay[0].T,
        head_norm_gain,
        closing_norm_gain[None],
    )
    return result[None]


def solution(mesh):
    placed = (
        P("pp", "fs", "tp"),
        P("pp", None, "tp"),
        P("pp", None, "tp"),
        P("pp", None, "tp"),
        P("pp", None, "tp"),
        P("pp", None, "tp"),
        P("pp", None, "tp"),
        P("pp", "tp"),
        P("pp", None, "tp"),
        P("pp", "tp"),
        P("tp"),
    )
    return jax.shard_map(
        functools.partial(on_device, mesh.shape["pp"], mesh.shape["tp"]),
        mesh=mesh,
        in_specs=placed,
        out_specs=P("pp", "fs", "tp"),
        check_vma=False,
    )
```

profile of v0, /device:TPU:17, one launch (start us, length us, event | category | flops | bytes accessed | tf_op | source)
XLA Modules:
  0.0 43.3 jit_solution(6601938415815602371)
XLA Ops:
  0.0 42.6 %shard_map.109 = bf16[128,512]{1,0:T(8,128)(2,1)S(1)} custom-call(bf16[128,512]{1,0:T(8,128)(2,1)} %bitcast.21, bf16[1024,512]{1,0:T(8,128)(2,1)} %bitcast.17, bf16[1024,512]{1,0:T(8,128)(2,1)} %bitcast.18, bf16[1024,512]{1,0:T(8,128)(2,1)} %bitcast.19, bf16[1024,512]{1,0:T(8,128)(2,1)} %bitcast.20, bf16[4,1024]{1,0:T(4,128)(2,1)} %bitcast.22, ...), custom_call_target="tpu_custom_call" | custom-call | tf_op jit(solution)/shard_map/pallas_call | solution.py:632
  42.6 0.7 %copy.13 = bf16[1,128,512]{2,1,0:T(8,128)(2,1)} copy(bf16[1,128,512]{2,1,0:T(8,128)(2,1)S(1)} %bitcast.16) | data formatting | bytes 262144
where the time goes:
time: 43.6 us; the launch traced here: 43.3 us
  Pallas kernels  42.6 us (98%)
  local copies, waits for them, and re-layouts  0.66 us (2%)
    pallas_call x1, Pallas kernels, on_device(): pl.pallas_call(functools.partial(stack_kernel, stages, group, size), out_...  42.6 us

commit v1 on v0

--- a/solution.py
+++ b/solution.py
@@ -86,10 +86,15 @@
         return lax.rem(core + d, group)
 
     barrier = pltpu.get_barrier_semaphore()
-    for d in range(1, stages):
-        pl.semaphore_signal(
-            barrier, inc=1, device_id={"pp": lax.rem(stage + d, stages)}, device_id_type=MESH
-        )
+
+    @pl.when(stage > 0)
+    def _():
+        pl.semaphore_signal(barrier, inc=1, device_id={"pp": stage - 1}, device_id_type=MESH)
+
+    @pl.when(stage < last)
+    def _():
+        pl.semaphore_signal(barrier, inc=1, device_id={"pp": stage + 1}, device_id_type=MESH)
+
     for d in others:
         pl.semaphore_signal(barrier, inc=1, device_id={"tp": peer(d)}, device_id_type=MESH)
 
@@ -130,8 +135,6 @@
     for load in loads:
         load.start()
 
-    pl.semaphore_wait(barrier, stages + group - 2)
-
     def entry_copy(h, span):
         return pltpu.make_async_remote_copy(
             src_ref=xout.at[stages, h, span],
@@ -172,32 +175,24 @@
             device_id_type=MESH,
         )
 
+    for h in range(heads):
+        token_copy(h, xout.at[stages, h]).wait()
+    pl.semaphore_wait(
+        barrier, group - 1 + (stage > 0).astype(jnp.int32) + (stage < last).astype(jnp.int32)
+    )
+
     @pl.when(stage == 0)
     def _():
-        for h in range(heads):
-            token_copy(h, xin.at[0, core * heads + h]).wait()
-
-    early = max(heads - 2, 0)
-
-    @pl.when(stage > 0)
-    def _():
-        for h in range(heads):
-            token_copy(h, xout.at[stages, h]).wait()
-
-        @pl.when(stage > 1)
-        def _():
-            pl.semaphore_wait(go_sem, 1)
-
         for span in spans:
             for h in range(heads):
+                for d in others:
+                    forward_copy(0, d, h, span).start()
+
+    @pl.when(stage == 1)
+    def _():
+        for span in spans:
+            for h in range(heads):
                 entry_copy(h, span).start()
-        entry_copy(early, spans[-1]).wait_send()
-
-        @pl.when(stage < last)
-        def _():
-            pl.semaphore_signal(
-                go_sem, inc=1, device_id={"pp": lax.rem(stage + 1, stages)}, device_id_type=MESH
-            )
 
     for load in small_loads:
         load.wait()
@@ -257,13 +252,19 @@
         return [dot(x, weights[i, own, :]) for i in range(4)]
 
     def begin(m, span):
-        x = gather(m, core, span)
-        squares, decay, beta = glance(x, core)
-        squares_own[span] = jnp.broadcast_to(squares, (size, width))
-        decay_own[span] = decay
-        beta_own[span] = beta
-        for i, a in enumerate(project(x, core)):
-            acc[i, span] = a
+        own = pl.ds(pl.multiple_of(core * half, half), half)
+
+        def first():
+            x = gather(m, core, span)
+            squares, decay, beta = glance(x, core)
+            squares_own[span] = jnp.broadcast_to(squares, (size, width))
+            decay_own[span] = decay
+            beta_own[span] = beta
+
+        def piece(i):
+            acc[i, span] = dot(gather(m, core, span), weights[i, own, :])
+
+        return [first] + [functools.partial(piece, i) for i in range(4)]
 
     def chunk(m, span, keep, use, between):
         squares = squares_own[span, :1]
@@ -278,8 +279,6 @@
             squares = squares + squares_other
             decay = decay + decay_other
             beta = beta + beta_other
-            for h in range(heads):
-                forward_copy(m, d, h, span).wait_send()
             mats = project(x, source)
             if d < group - 1:
                 for i in range(4):
@@ -433,7 +432,12 @@
                     axis=0,
                 ).astype(BF16)
             )
-        between()
+        queue = between()
+
+        def fill(count):
+            for _ in range(min(count, len(queue))):
+                queue.pop(0)()
+
         update = [dot(inverse[g], apart([a.astype(BF16) for a in values], g)) for g in every]
 
         def split(wide):
@@ -448,6 +452,7 @@
                 dot(inverse[g], stacked(jnp.where(outside, system[g], 0.0).astype(BF16)))
                 for g in every
             ]
+            fill(2)
             sign = -1.0
             done = 1
             while done < pieces:
@@ -460,8 +465,10 @@
                 sign = 1.0
                 if done < pieces:
                     chain = [dot(rounded[g], stacked(rounded[g])) for g in every]
+                fill(1)
         final = split(update)
         mixed = [dot(scores[g], apart(final, g)) for g in every]
+        fill(len(queue))
         if use:
             mixed = [mixed[g] + before[g][size:] for g in every]
         for h in range(heads):
@@ -486,17 +493,6 @@
             for d in others:
                 forward_copy(m, d, h, span).start()
 
-    def enter(span):
-        @pl.when(stage > 0)
-        def _():
-            arrive(0, span)
-
-        @pl.when(stage == 0)
-        def _():
-            for h in range(heads):
-                for d in others:
-                    forward_copy(0, d, h, span).start()
-
     def leave(m, span):
         @pl.when(stage < last)
         def _():
@@ -526,23 +522,35 @@
                     def _():
                         arrive(following, ahead)
 
-                begin(following, ahead)
+                return begin(following, ahead)
 
             chunk(m, span, keep=i + 1 < len(spans), use=i > 0, between=between)
             leave(m, span)
         return 0
 
-    enter(spans[0])
-    for load in loads:
-        load.wait()
-    begin(0, spans[0])
-
-    @pl.when(stage == 0)
-    def _():
-        for span in spans[1:]:
-            for h in range(heads):
-                for d in others:
-                    forward_copy(0, d, h, span).start()
+    @pl.when(stage > 1)
+    def _():
+        pl.semaphore_wait(go_sem, 1)
+        for span in spans:
+            for h in range(heads):
+                entry_copy(h, span).start()
+
+    @pl.when(stage > 0)
+    def _():
+        entry_copy(heads - 1, spans[0]).wait_send()
+
+    @pl.when((stage > 0) & (stage < last))
+    def _():
+        pl.semaphore_signal(go_sem, inc=1, device_id={"pp": stage + 1}, device_id_type=MESH)
+
+    @pl.when(stage > 0)
+    def _():
+        arrive(0, spans[0])
+
+    for i, piece in enumerate(begin(0, spans[0])):
+        if i > 0:
+            loads[i - 1].wait()
+        piece()
 
     lax.fori_loop(0, stages, step, 0)
 
@@ -578,10 +586,15 @@
     def _():
         for span in spans:
             for h in range(heads):
-                if h != early or span is not spans[-1]:
+                if h < heads - 1 or span is not spans[0]:
                     entry_copy(h, span).wait_send()
 
     def drain(m, _):
+        for span in spans:
+            for h in range(heads):
+                for d in others:
+                    forward_copy(m, d, h, span).wait_send()
+
         @pl.when((stage < last) | (m < last))
         def _():
             for span in spans:

time: 43.6 us -> 39 us (0.89)
  Pallas kernels: 42.6 us -> 38.2 us
    pallas_call x1, Pallas kernels: 42.6 us -> 38.2 us  [on_device(): pl.pallas_call(functools.partial(stack_kernel, stages, group, size), out_...]
where the time goes in v1:
time: 39 us; the launch traced here: 38.9 us
  Pallas kernels  38.2 us (98%)
  local copies, waits for them, and re-layouts  0.66 us (2%)
    pallas_call x1, Pallas kernels, on_device(): pl.pallas_call(functools.partial(stack_kernel, stages, group, size), out_...  38.2 us

profile of v1, /device:TPU:17, one launch (start us, length us, event | category | flops | bytes accessed | tf_op | source)
XLA Modules:
  0.0 38.9 jit_solution(2862446627795238400)
XLA Ops:
  0.0 38.2 %shard_map.109 = bf16[128,512]{1,0:T(8,128)(2,1)S(1)} custom-call(bf16[128,512]{1,0:T(8,128)(2,1)} %bitcast.21, bf16[1024,512]{1,0:T(8,128)(2,1)} %bitcast.17, bf16[1024,512]{1,0:T(8,128)(2,1)} %bitcast.18, bf16[1024,512]{1,0:T(8,128)(2,1)} %bitcast.19, bf16[1024,512]{1,0:T(8,128)(2,1)} %bitcast.20, bf16[4,1024]{1,0:T(4,128)(2,1)} %bitcast.22, ...), custom_call_target="tpu_custom_call" | custom-call | tf_op jit(solution)/shard_map/pallas_call | solution.py:645
  38.2 0.7 %copy.13 = bf16[1,128,512]{2,1,0:T(8,128)(2,1)} copy(bf16[1,128,512]{2,1,0:T(8,128)(2,1)S(1)} %bitcast.16) | data formatting | bytes 262144

commit v2 on v1

--- a/solution.py
+++ b/solution.py
@@ -535,21 +535,25 @@
             for h in range(heads):
                 entry_copy(h, span).start()
 
+    @pl.when(stage == 1)
+    def _():
+        entry_copy(1, spans[0]).wait_send()
+
+    @pl.when(stage > 1)
+    def _():
+        entry_copy(1, spans[-1]).wait_send()
+
+    @pl.when((stage > 0) & (stage < last))
+    def _():
+        pl.semaphore_signal(go_sem, inc=1, device_id={"pp": stage + 1}, device_id_type=MESH)
+
     @pl.when(stage > 0)
     def _():
-        entry_copy(heads - 1, spans[0]).wait_send()
-
-    @pl.when((stage > 0) & (stage < last))
-    def _():
-        pl.semaphore_signal(go_sem, inc=1, device_id={"pp": stage + 1}, device_id_type=MESH)
-
-    @pl.when(stage > 0)
-    def _():
         arrive(0, spans[0])
 
-    for i, piece in enumerate(begin(0, spans[0])):
-        if i > 0:
-            loads[i - 1].wait()
+    for load in loads:
+        load.wait()
+    for piece in begin(0, spans[0]):
         piece()
 
     lax.fori_loop(0, stages, step, 0)
@@ -586,7 +590,12 @@
     def _():
         for span in spans:
             for h in range(heads):
-                if h < heads - 1 or span is not spans[0]:
+                f1 = h == 1 and span is spans[0]
+                f2 = h == 1 and span is spans[-1]
+                wanted = (not f1) if f1 == f2 else (jnp.where(stage == 1, int(not f1), int(not f2)) == 1)
+
+                @pl.when(wanted)
+                def _(h=h, span=span):
                     entry_copy(h, span).wait_send()
 
     def drain(m, _):

time: 39 us -> 38.4 us (0.985)
  Pallas kernels: 38.2 us -> 37.5 us
    pallas_call x1, Pallas kernels: 38.2 us -> 37.5 us  [on_device(): pl.pallas_call(functools.partial(stack_kernel, stages, group, size), out_...]
where the time goes in v2:
time: 38.4 us; the launch traced here: 38.2 us
  Pallas kernels  37.5 us (98%)
  local copies, waits for them, and re-layouts  0.66 us (2%)
    pallas_call x1, Pallas kernels, on_device(): pl.pallas_call(functools.partial(stack_kernel, stages, group, size), out_...  37.5 us

profile of v2, /device:TPU:17, one launch (start us, length us, event | category | flops | bytes accessed | tf_op | source)
XLA Modules:
  0.0 38.2 jit_solution(11427569640521904941)
XLA Ops:
  0.0 37.5 %shard_map.109 = bf16[128,512]{1,0:T(8,128)(2,1)S(1)} custom-call(bf16[128,512]{1,0:T(8,128)(2,1)} %bitcast.21, bf16[1024,512]{1,0:T(8,128)(2,1)} %bitcast.17, bf16[1024,512]{1,0:T(8,128)(2,1)} %bitcast.18, bf16[1024,512]{1,0:T(8,128)(2,1)} %bitcast.19, bf16[1024,512]{1,0:T(8,128)(2,1)} %bitcast.20, bf16[4,1024]{1,0:T(4,128)(2,1)} %bitcast.22, ...), custom_call_target="tpu_custom_call" | custom-call | tf_op jit(solution)/shard_map/pallas_call | solution.py:654
  37.6 0.7 %copy.13 = bf16[1,128,512]{2,1,0:T(8,128)(2,1)} copy(bf16[1,128,512]{2,1,0:T(8,128)(2,1)S(1)} %bitcast.16) | data formatting | bytes 262144

commit v3 on v2

--- a/solution.py
+++ b/solution.py
@@ -264,7 +264,7 @@
         def piece(i):
             acc[i, span] = dot(gather(m, core, span), weights[i, own, :])
 
-        return [first] + [functools.partial(piece, i) for i in range(4)]
+        return [functools.partial(piece, 0), first] + [functools.partial(piece, i) for i in range(1, 4)]
 
     def chunk(m, span, keep, use, between):
         squares = squares_own[span, :1]
@@ -467,6 +467,7 @@
                     chain = [dot(rounded[g], stacked(rounded[g])) for g in every]
                 fill(1)
         final = split(update)
+        fill(1)
         mixed = [dot(scores[g], apart(final, g)) for g in every]
         fill(len(queue))
         if use:
@@ -563,28 +564,30 @@
         for h in range(heads):
             yin[h] = xout[last, h]
 
-    @pl.when(stage < last)
-    def _():
-        for span in spans:
-            for h in range(heads):
-                exit_copy(0, h, span).wait_recv()
-
-    final = [yin[h].astype(F32) for h in range(heads)]
-    total = sum(jnp.sum(a * a, axis=1, keepdims=True) for a in final)
-    part_mine[...] = jnp.broadcast_to(total, part_mine.shape)
-    part_copies = [
-        pltpu.make_async_remote_copy(
-            src_ref=part_mine,
-            dst_ref=part_other.at[d - 1],
-            send_sem=part_send.at[d - 1],
-            recv_sem=part_recv.at[d - 1],
+    def part_copy(d, span):
+        at = span.start // size
+        return pltpu.make_async_remote_copy(
+            src_ref=part_mine.at[span],
+            dst_ref=part_other.at[d - 1, span],
+            send_sem=part_send.at[d - 1, at],
+            recv_sem=part_recv.at[d - 1, at],
             device_id={"tp": peer(d)},
             device_id_type=MESH,
         )
-        for d in others
-    ]
-    for copy in part_copies:
-        copy.start()
+
+    for span in spans:
+
+        @pl.when(stage < last)
+        def _(span=span):
+            for h in range(heads):
+                exit_copy(0, h, span).wait_recv()
+
+        final = [yin[h, span].astype(F32) for h in range(heads)]
+        total = sum(a * a for a in final)
+        total = jnp.sum(total, axis=1, keepdims=True)
+        part_mine[span] = jnp.broadcast_to(total, (size, width))
+        for d in others:
+            part_copy(d, span).start()
 
     @pl.when(stage > 0)
     def _():
@@ -613,15 +616,16 @@
         return 0
 
     lax.fori_loop(0, stages, drain, 0)
-    total = part_mine[...]
-    for copy in part_copies:
-        copy.wait()
-    for d in others:
-        total = total + part_other[d - 1]
-    inv_rms = lax.rsqrt(total / model_width + epsilon)
-    for h in range(heads):
-        part = slice(h * width, (h + 1) * width)
-        out[:, part] = (final[h] * inv_rms * closing_gain[:, part]).astype(BF16)
+    for span in spans:
+        total = part_mine[span]
+        for d in others:
+            part_copy(d, span).wait()
+            total = total + part_other[d - 1, span]
+        inv_rms = lax.rsqrt(total / model_width + epsilon)
+        for h in range(heads):
+            part = slice(h * width, (h + 1) * width)
+            scaled = yin[h, span].astype(F32) * inv_rms * closing_gain[:, part]
+            out[span, part] = scaled.astype(BF16)
 
 
 def on_device(
@@ -689,8 +693,8 @@
             dma((stages, group - 1, parts, heads)),
             dma((stages, parts, heads)),
             dma((parts, heads)),
-            dma((group - 1,)),
-            dma((group - 1,)),
+            dma((group - 1, parts)),
+            dma((group - 1, parts)),
         ],
         compiler_params=pltpu.CompilerParams(
             collective_id=0, has_side_effects=True, vmem_limit_bytes=60 * 1024 * 1024

time: 38.4 us -> 38.2 us (level)
  no operation moved by 1% of the time
where the time goes in v3:
time: 38.2 us; the launch traced here: 38 us
  Pallas kernels  37.4 us (98%)
  local copies, waits for them, and re-layouts  0.66 us (2%)
    pallas_call x1, Pallas kernels, on_device(): pl.pallas_call(functools.partial(stack_kernel, stages, group, size), out_...  37.4 us

profile of v3, /device:TPU:17, one launch (start us, length us, event | category | flops | bytes accessed | tf_op | source)
XLA Modules:
  0.0 38.0 jit_solution(7000999219896821158)
XLA Ops:
  0.0 37.4 %shard_map.109 = bf16[128,512]{1,0:T(8,128)(2,1)S(1)} custom-call(bf16[128,512]{1,0:T(8,128)(2,1)} %bitcast.21, bf16[1024,512]{1,0:T(8,128)(2,1)} %bitcast.17, bf16[1024,512]{1,0:T(8,128)(2,1)} %bitcast.18, bf16[1024,512]{1,0:T(8,128)(2,1)} %bitcast.19, bf16[1024,512]{1,0:T(8,128)(2,1)} %bitcast.20, bf16[4,1024]{1,0:T(4,128)(2,1)} %bitcast.22, ...), custom_call_target="tpu_custom_call" | custom-call | tf_op jit(solution)/shard_map/pallas_call | solution.py:658
  37.4 0.7 %copy.13 = bf16[1,128,512]{2,1,0:T(8,128)(2,1)} copy(bf16[1,128,512]{2,1,0:T(8,128)(2,1)S(1)} %bitcast.16) | data formatting | bytes 262144

commit v4 on v3

--- a/solution.py
+++ b/solution.py
@@ -57,6 +57,7 @@
     past_key,
     past_value,
     past_fade,
+    part_exit,
     part_mine,
     part_other,
     w_sem,
@@ -71,6 +72,7 @@
     y_recv,
     part_send,
     part_recv,
+    exit_sem,
 ):
     stage = lax.axis_index("pp")
     core = lax.axis_index("tp")
@@ -494,6 +496,16 @@
             for d in others:
                 forward_copy(m, d, h, span).start()
 
+    def exit_part(d):
+        return pltpu.make_async_remote_copy(
+            src_ref=part_exit,
+            dst_ref=part_other.at[d - 1, spans[-1]],
+            send_sem=exit_sem.at[d - 1],
+            recv_sem=part_recv.at[d - 1, len(spans) - 1],
+            device_id={"pp": last - 1, "tp": peer(d)},
+            device_id_type=MESH,
+        )
+
     def leave(m, span):
         @pl.when(stage < last)
         def _():
@@ -527,6 +539,17 @@
 
             chunk(m, span, keep=i + 1 < len(spans), use=i > 0, between=between)
             leave(m, span)
+
+            if i + 1 == len(spans):
+
+                @pl.when((stage == last) & (m == last - 1))
+                def _(span=span):
+                    rows = [xout[m, h, span].astype(F32) for h in range(heads)]
+                    total = jnp.sum(sum(a * a for a in rows), axis=1, keepdims=True)
+                    part_exit[...] = jnp.broadcast_to(total, (size, width))
+                    for d in others:
+                        exit_part(d).start()
+
         return 0
 
     @pl.when(stage > 1)
@@ -586,8 +609,12 @@
         total = sum(a * a for a in final)
         total = jnp.sum(total, axis=1, keepdims=True)
         part_mine[span] = jnp.broadcast_to(total, (size, width))
-        for d in others:
-            part_copy(d, span).start()
+        told = (stage == last - 1) if span is spans[-1] else (stage < 0)
+
+        @pl.when(jnp.logical_not(told))
+        def _(span=span):
+            for d in others:
+                part_copy(d, span).start()
 
     @pl.when(stage > 0)
     def _():
@@ -616,10 +643,23 @@
         return 0
 
     lax.fori_loop(0, stages, drain, 0)
+    @pl.when(stage == last)
+    def _():
+        for d in others:
+            exit_part(d).wait_send()
+
+    for span in spans:
+        told = (stage == last - 1) if span is spans[-1] else (stage < 0)
+
+        @pl.when(jnp.logical_not(told))
+        def _(span=span):
+            for d in others:
+                part_copy(d, span).wait_send()
+
     for span in spans:
         total = part_mine[span]
         for d in others:
-            part_copy(d, span).wait()
+            part_copy(d, span).wait_recv()
             total = total + part_other[d - 1, span]
         inv_rms = lax.rsqrt(total / model_width + epsilon)
         for h in range(heads):
@@ -681,6 +721,7 @@
             pltpu.VMEM((heads, size, width), BF16),
             pltpu.VMEM((heads, size, width), BF16),
             pltpu.VMEM((8, length), F32),
+            pltpu.VMEM((size, width), F32),
             pltpu.VMEM((length, width), F32),
             pltpu.VMEM((group - 1, length, width), F32),
             dma((4,)),
@@ -695,6 +736,7 @@
             dma((parts, heads)),
             dma((group - 1, parts)),
             dma((group - 1, parts)),
+            dma((group - 1,)),
         ],
         compiler_params=pltpu.CompilerParams(
             collective_id=0, has_side_effects=True, vmem_limit_bytes=60 * 1024 * 1024

time: 38.2 us -> 37.7 us (0.987)
  Pallas kernels: 37.4 us -> 36.6 us
    pallas_call x1, Pallas kernels: 37.4 us -> 36.6 us  [on_device(): pl.pallas_call(functools.partial(stack_kernel, stages, group, size), out_...]
where the time goes in v4:
time: 37.7 us; the launch traced here: 37.3 us
  Pallas kernels  36.6 us (97%)
  local copies, waits for them, and re-layouts  0.66 us (2%)
    pallas_call x1, Pallas kernels, on_device(): pl.pallas_call(functools.partial(stack_kernel, stages, group, size), out_...  36.6 us

profile of v4, /device:TPU:17, one launch (start us, length us, event | category | flops | bytes accessed | tf_op | source)
XLA Modules:
  0.0 37.3 jit_solution(292610026489021407)
XLA Ops:
  0.0 36.6 %shard_map.109 = bf16[128,512]{1,0:T(8,128)(2,1)S(1)} custom-call(bf16[128,512]{1,0:T(8,128)(2,1)} %bitcast.21, bf16[1024,512]{1,0:T(8,128)(2,1)} %bitcast.17, bf16[1024,512]{1,0:T(8,128)(2,1)} %bitcast.18, bf16[1024,512]{1,0:T(8,128)(2,1)} %bitcast.19, bf16[1024,512]{1,0:T(8,128)(2,1)} %bitcast.20, bf16[4,1024]{1,0:T(4,128)(2,1)} %bitcast.22, ...), custom_call_target="tpu_custom_call" | custom-call | tf_op jit(solution)/shard_map/pallas_call | solution.py:698
  36.6 0.7 %copy.13 = bf16[1,128,512]{2,1,0:T(8,128)(2,1)} copy(bf16[1,128,512]{2,1,0:T(8,128)(2,1)S(1)} %bitcast.16) | data formatting | bytes 262144
